TPU v7x, 32 devices: a whole 2x2x4 slice. The times are simulated.
32 devices in a mesh: grp: 1, sp: 8 (over z, core), tp: 4 (over y, x).
Axes of the slice: x: 2, y: 2, z: 4, core: 2. Of those that a mesh axis runs over, the one named last changes fastest.
Arguments:
- queries: bfloat16 [2048, 16, 128], P(('grp', 'sp'), 'tp'), may hold values from -6 to 6
- keys: bfloat16 [2048, 4, 128], P(('grp', 'sp'), 'tp'), may hold values from -6 to 6
- values: bfloat16 [2048, 4, 128], P(('grp', 'sp'), 'tp'), may hold values from -6 to 6
- log_gates: float32 [16, 2048], P('tp', ('grp', 'sp')), may hold values from -260 to 0, as said below
- documents: int32 [2048], P(('grp', 'sp')), may hold values from 0 to 2, never falling along the last dimension, each value on 1 to 1536 neighbouring positions
- query_gain: float32 [128], replicated, may hold values from 0.5 to 5
- key_gain: float32 [128], replicated, may hold values from 0.5 to 5
- out_weight: bfloat16 [2048, 2048], P('tp'), may hold values from -0.125 to 0.125
- residual: bfloat16 [2048, 2048], P(('grp', 'sp', 'tp')), may hold values from -1.5 to 1.5
- norm_gain: float32 [2048], replicated, may hold values from 0.1 to 1.9
- routes: int32 [2048, 2], P(('grp', 'sp', 'tp')), may hold values from 0 to 3, all different within a row; in each aligned block of 64 rows (0 to 63, 64 to 127, ...) at most 48 rows name the same one
- route_weights: float32 [2048, 2], P(('grp', 'sp', 'tp')), may hold values from 0.1 to 1
- w_gate: bfloat16 [8, 2048, 2048], P('sp', None, 'tp'), may hold values from -0.125 to 0.125
- w_up: bfloat16 [8, 2048, 2048], P('sp', None, 'tp'), may hold values from -0.125 to 0.125
- w_down: bfloat16 [8, 2048, 2048], P('sp', 'tp'), may hold values from -0.09375 to 0.09375
Outputs:
- layer_out: bfloat16 [2048, 2048], P(('grp', 'sp', 'tp'))
Inputs may be any that keep to these rules, and one draw needn't show every extreme that they name: `log_gates`: non-increasing along positions for every head. `documents`: never falls along positions. `routes`: the 2 experts of a token differ; among the 64 tokens of one device (aligned blocks) no expert is named by more than 48 tokens, and in every draw some expert is named by exactly 48 of them.
All inputs are finite; a program needn't handle non-finite values.
Results may differ from a plain program's by a relative error of at most 0.017.
The roundings to bfloat16 on the way count: a program that leaves them out, or rounds other values in their place, can miss the bound.
Values may be sent and summed in bfloat16 or wider, within the bound.
A program may use at most 128 MiB of HBM per device.

v0:
```python
import jax
import jax.numpy as jnp
from jax import lax
from jax.sharding import PartitionSpec as P

EPSILON = 1e-06
FLOOR = -1e30


def rms_scale(inputs, gain):
    return inputs * lax.rsqrt(jnp.mean(inputs * inputs, axis=-1, keepdims=True) + EPSILON) * gain


def local(
    queries,
    keys,
    values,
    log_gates,
    documents,
    query_gain,
    key_gain,
    out_weight,
    residual,
    norm_gain,
    routes,
    route_weights,
    w_gate,
    w_up,
    w_down,
):
    tok_dev, local_heads, head_size = queries.shape
    seq_index = lax.axis_index("sp")
    offset = seq_index * tok_dev
    query_norm = (rms_scale(queries.astype(jnp.float32), query_gain) * head_size ** (-0.5)).astype(
        jnp.bfloat16
    )
    key_norm = rms_scale(keys[:, 0, :].astype(jnp.float32), key_gain).astype(jnp.bfloat16)
    value_rows = values[:, 0, :]
    doc_float = documents.astype(jnp.float32)
    gates_all, docs_all = (
        lax.all_gather(log_gates, "sp", axis=1, tiled=True),
        lax.all_gather(doc_float[None, :], "sp", axis=1, tiled=True),
    )
    query_pos = offset + jnp.arange(tok_dev, dtype=jnp.int32)
    first_doc = doc_float[0]
    last_pos = offset + tok_dev - 1
    start_state = (
        jnp.full((local_heads, tok_dev), FLOOR, jnp.float32),
        jnp.zeros((local_heads, tok_dev), jnp.float32),
        jnp.zeros((local_heads, tok_dev, head_size), jnp.float32),
    )
    key_piece = lax.all_gather(key_norm, "sp", axis=0, tiled=True)
    value_piece = lax.all_gather(value_rows, "sp", axis=0, tiled=True)
    piece_rows = key_piece.shape[0]
    block_rows = 512
    block_count = piece_rows // block_rows

    def one_block(running, block_index):
        local_start = block_index * block_rows
        block_keys = lax.dynamic_slice_in_dim(key_piece, local_start, block_rows, 0)
        block_values = lax.dynamic_slice_in_dim(value_piece, local_start, block_rows, 0)
        block_gates = lax.dynamic_slice_in_dim(gates_all, local_start, block_rows, 1)
        block_docs = lax.dynamic_slice_in_dim(docs_all, local_start, block_rows, 1)[0]
        needed = (local_start <= last_pos) & (block_docs[block_rows - 1] >= first_doc)

        def update(current):
            running_max, running_sum, running_out = current
            scores = jnp.einsum(
                "qhd,kd->hqk", query_norm, block_keys, preferred_element_type=jnp.float32
            )
            scores = scores + log_gates[:, :, None] - block_gates[:, None, :]
            key_pos = local_start + jnp.arange(block_rows, dtype=jnp.int32)
            allowed = (key_pos[None, :] <= query_pos[:, None]) & (
                block_docs[None, :] == doc_float[:, None]
            )
            scores = jnp.where(allowed[None], scores, -jnp.inf)
            new_max = jnp.maximum(running_max, jnp.max(scores, axis=-1))
            expo = jnp.exp(scores - new_max[..., None])
            factor = jnp.exp(running_max - new_max)
            new_sum = factor * running_sum + jnp.sum(expo, axis=-1)
            added = jnp.einsum(
                "hqk,kd->hqd",
                expo.astype(jnp.bfloat16),
                block_values,
                preferred_element_type=jnp.float32,
            )
            return (new_max, new_sum, factor[..., None] * running_out + added)

        def keep(current):
            return current

        return (lax.cond(needed, update, keep, running), None)

    result, _ = lax.scan(one_block, start_state, jnp.arange(block_count, dtype=jnp.int32))
    final_max, final_sum, final_out = result
    attended = (final_out / final_sum[..., None]).astype(jnp.bfloat16)
    attended = jnp.transpose(attended, (1, 0, 2)).reshape(tok_dev, local_heads * head_size)
    n_sp = lax.axis_size("sp")
    n_tp = lax.axis_size("tp")
    rows_dev = tok_dev // n_tp
    projected = lax.psum_scatter(
        jnp.dot(attended, out_weight, preferred_element_type=jnp.float32).astype(jnp.bfloat16),
        "tp",
        scatter_dimension=0,
        tiled=True,
    ).astype(jnp.float32)
    mixed = (residual.astype(jnp.float32) + projected).astype(jnp.bfloat16)
    normed = rms_scale(mixed.astype(jnp.float32), norm_gain).astype(jnp.bfloat16)
    model_dim = normed.shape[1]
    experts = n_sp // 2
    capacity = min(rows_dev, 6 * rows_dev // n_sp)
    expert_ids = jnp.arange(experts, dtype=jnp.int32)
    chosen = routes[:, :, None] == expert_ids[None, None, :]
    picked = jnp.sum(chosen.astype(jnp.float32), axis=1)
    weight_of = jnp.sum(jnp.where(chosen, route_weights[:, :, None], 0.0), axis=1)
    rank = jnp.cumsum(picked, axis=0) - 1.0
    slot_ids = jnp.arange(capacity).astype(jnp.float32)
    placing = picked.T[:, None, :] * (rank.T[:, None, :] == slot_ids[None, :, None]).astype(
        jnp.float32
    )
    outgoing = jnp.einsum(
        "ecr,rd->ecd", placing.astype(jnp.bfloat16), normed, preferred_element_type=jnp.float32
    ).astype(jnp.bfloat16)
    outgoing = jnp.repeat(outgoing, 2, axis=0)
    gate_rows = w_gate[0]
    up_rows = w_up[0]
    down_rows = w_down[0]
    arrived = lax.all_gather(
        lax.all_to_all(outgoing, "sp", split_axis=0, concat_axis=0, tiled=True),
        "tp",
        axis=0,
        tiled=True,
    )
    lead, items, width = arrived.shape
    flat = arrived.reshape(lead * items, width)
    gate_act = jnp.dot(flat, gate_rows, preferred_element_type=jnp.float32)
    up_act = jnp.dot(flat, up_rows, preferred_element_type=jnp.float32)
    hidden = (jax.nn.silu(gate_act) * up_act).astype(jnp.bfloat16)
    partial_out = jnp.dot(hidden, down_rows, preferred_element_type=jnp.float32).astype(
        jnp.bfloat16
    )
    partial_all = partial_out.reshape(lead, items, width)
    summed = lax.psum_scatter(
        partial_all.astype(jnp.float32).astype(jnp.bfloat16), "tp", scatter_dimension=0, tiled=True
    ).astype(jnp.float32)
    returned = lax.all_to_all(
        summed.astype(jnp.bfloat16), "sp", split_axis=0, concat_axis=0, tiled=True
    ).astype(summed.dtype)
    results = jnp.sum(returned.reshape(experts, 2, capacity, model_dim), axis=1)
    combining = placing * weight_of.T[:, None, :]
    routed = jnp.einsum("ecr,ecd->rd", combining, results, precision=lax.Precision.HIGHEST)
    return (mixed.astype(jnp.float32) + routed).astype(jnp.bfloat16)


def solution(mesh):
    return jax.shard_map(
        local,
        mesh=mesh,
        in_specs=(
            P(("grp", "sp"), "tp", None),
            P(("grp", "sp"), "tp", None),
            P(("grp", "sp"), "tp", None),
            P("tp", ("grp", "sp")),
            P(("grp", "sp")),
            P(),
            P(),
            P("tp", None),
            P(("grp", "sp", "tp"), None),
            P(),
            P(("grp", "sp", "tp"), None),
            P(("grp", "sp", "tp"), None),
            P("sp", None, "tp"),
            P("sp", None, "tp"),
            P("sp", "tp", None),
        ),
        out_specs=P(("grp", "sp", "tp"), None),
        check_vma=False,
    )
```

profile of v0, /device:TPU:0, one launch (start us, length us, event | category | flops | bytes accessed | tf_op | source)
XLA Modules:
  0.0 380.4 jit_solution(16620844591719439829)
XLA Ops:
  6.5 0.8 convert_element_type.80
  7.4 0.6 slice.7
  8.0 0.9 fusion.34
  8.9 1.2 fusion.23
  10.1 13.5 %all-gather.2 = f32[8,1,256]{2,1,0:T(1,128)S(1)} all-gather(f32[1,1,256]{2,1,0:T(1,128)S(1)} %bitcast.73), channel_id=2, replica_groups=mesh['grp'=1,'sp'=8,'tp'=4] {'sp'}, dimensions={0}, use_global_device_ids=true | all-gather | bytes 9216 | tf_op jit(solution)/shard_map/all_gather | solution.py:42
  23.6 14.2 %all_gather.17 = f32[4,2048]{1,0:T(4,128)S(1)} all-gather(f32[4,256]{1,0:T(4,128)} %param.22), channel_id=1, replica_groups=mesh['grp'=1,'sp'=8,'tp'=4] {'sp'}, dimensions={1}, use_global_device_ids=true | all-gather | bytes 36864 | tf_op jit(solution)/shard_map/all_gather | solution.py:41
  37.8 0.9 fusion.36
  38.8 15.8 %all_gather.16 = bf16[2048,128]{1,0:T(8,128)(2,1)} all-gather(bf16[256,128]{1,0:T(8,128)(2,1)S(1)} %fusion.36), channel_id=1, replica_groups=mesh['grp'=1,'sp'=8,'tp'=4] {'sp'}, dimensions={0}, use_global_device_ids=true | all-gather | bytes 589824 | tf_op jit(solution)/shard_map/all_gather | solution.py:52
  54.6 15.1 %all-gather.1 = bf16[2048,1,128]{2,0,1:T(8,128)(2,1)S(1)} all-gather(bf16[256,1,128]{2,0,1:T(8,128)(2,1)} %param.21), channel_id=3, replica_groups=mesh['grp'=1,'sp'=8,'tp'=4] {'sp'}, dimensions={0}, use_global_device_ids=true | all-gather | bytes 589824 | tf_op jit(solution)/shard_map/all_gather | solution.py:53
  69.7 1.2 fusion.26
  70.9 15.6 %while.15 = (s32[]{:T(128)}, f32[4,256]{1,0:T(4,128)S(1)}, f32[4,256]{1,0:T(4,128)S(1)}, f32[4,256,128]{2,1,0:T(8,128)S(1)}, s32[4]{0:T(128)S(1)}, /*index=5*/s3...) while((s32[]{:T(128)}, f32[4,256]{1,0:T(4,128)S(1)}, ...), condition=%wide.region_7.8_spmd.clone, body=%wide.region_2.7_spmd.clone.sunk | while | flops 273287936 | bytes 8237029 | solution.py:94
  70.9 0.7 dynamic_slice.48
  72.3 0.6 constant_dynamic-slice_fusion.5
  74.1 2.9 conditional.3
  74.1 0.1 constant_dynamic-slice_fusion
  74.2 0.2 compare_and_fusion
  74.4 1.5 fusion.49
  75.9 0.3 fusion.5
  76.2 0.7 convolution_add_fusion
  77.0 0.7 dynamic_slice.48
  78.3 0.6 constant_dynamic-slice_fusion.5
  80.2 0.7 dynamic_slice.48
  81.5 0.6 constant_dynamic-slice_fusion.5
  83.4 0.7 dynamic_slice.48
  84.7 0.6 constant_dynamic-slice_fusion.5
  86.6 0.2 copy.38
  86.9 3.4 convolution_convert_fusion.1
  90.2 0.0 reduce-scatter.3.cloned.1.call-update
  90.2 0.0 all-gather.5.cloned.1.call-start
  90.3 0.1 copy.39
  90.4 0.1 reduce_window_sum.11
  90.5 0.1 copy.40
  90.6 34.4 %reduce-scatter.3.cloned.1.call-done = bf16[64,2048]{1,0:T(8,128)(2,1)} async-done(((bf16[256,2048]{1,0:T(8,128)(2,1)}), bf16[64,2048]{1,0:T(8,128)(2,1)}) %reduce-scatter.3.cloned.1.call-update) | async-done | bytes 262160 | tf_op jit(solution)/shard_map/reduce_scatter | solution.py:101
  125.0 1.1 fusion.27
  126.2 1.4 convolution_convert_fusion.2
  127.5 0.2 broadcast_in_dim.72
  127.7 42.3 %all_to_all.10 = bf16[8,48,2048]{2,1,0:T(8,128)(2,1)} all-to-all(bf16[8,48,2048]{2,1,0:T(8,128)(2,1)S(1)} %bitcast.69), channel_id=1, replica_groups=mesh['grp'=1,'sp'=8,'tp'=4] {'sp'}, dimensions={0} | all-to-all | bytes 3145728 | tf_op jit(solution)/shard_map/all_to_all | solution.py:129
  170.0 0.0 all-gather.5.cloned.1.call-update
  170.1 0.0 reduce-scatter.5.cloned.1.call-start
  170.1 68.1 %all-gather.5.cloned.1.call-done = bf16[32,48,2048]{2,1,0:T(8,128)(2,1)} async-done(((bf16[8,48,2048]{2,1,0:T(8,128)(2,1)}), bf16[32,48,2048]{2,1,0:T(8,128)(2,1)}) %all-gather.5.cloned.1.call-update) | async-done | bytes 6291472 | tf_op jit(solution)/shard_map/all_gather | solution.py:128
  238.2 8.5 %fusion.19 = f32[1536,512]{1,0:T(8,128)} fusion(bf16[1536,2048]{1,0:T(8,128)(2,1)} %bitcast.78, bf16[1,2048,512]{2,1,0:T(8,128)(2,1)} %param.31), kind=kOutput, calls=%fused_computation.34 | convolution fusion | flops 3221225472 | bytes 11534336 | tf_op jit(solution)/shard_map/dot_general | solution.py:136
  246.7 11.8 %convolution_convert_fusion = bf16[1536,2048]{1,0:T(8,128)(2,1)} fusion(bf16[1,512,2048]{2,1,0:T(8,128)(2,1)S(1)} %copy-done, bf16[1536,2048]{1,0:T(8,128)(2,1)} %bitcast.79, f32[1536,512]{1,0:T(8,128)} %fusion.19, bf16[1,2048,512]{2,1,0:T(8,128)(2,1)} %param.32), kind=kOutput, calls=%fused_computation.23 | convolution fusion | flops 6450315264 | bytes 19922944 | tf_op jit(solution)/shard_map/dot_general | solution.py:139
  258.5 0.0 reduce-scatter.5.cloned.1.call-update
  258.5 70.1 %reduce-scatter.5.cloned.1.call-done = bf16[8,48,2048]{2,1,0:T(8,128)(2,1)} async-done(((bf16[32,48,2048]{2,1,0:T(8,128)(2,1)}), bf16[8,48,2048]{2,1,0:T(8,128)(2,1)}) %reduce-scatter.5.cloned.1.call-update) | async-done | bytes 1572880 | tf_op jit(solution)/shard_map/reduce_scatter | solution.py:143
  328.7 42.4 %all_to_all.11 = bf16[8,48,2048]{2,1,0:T(8,128)(2,1)S(1)} all-to-all(bf16[8,48,2048]{2,1,0:T(8,128)(2,1)} %reduce-scatter.5.cloned.1.call-done), channel_id=1, replica_groups=mesh['grp'=1,'sp'=8,'tp'=4] {'sp'}, dimensions={0} | all-to-all | bytes 3145728 | tf_op jit(solution)/shard_map/all_to_all | solution.py:146
  371.1 0.3 convert_reduce_fusion
  371.4 0.6 copy-done.2
  372.0 1.9 fusion.16
  (41 shorter events, 0.3 us)
Async XLA Ops:
  6.5 240.2 %copy-start = (bf16[1,512,2048]{2,1,0:T(8,128)(2,1)S(1)}, bf16[1,512,2048]{2,1,0:T(8,128)(2,1)}, u32[]{:S(2)}) copy-start(bf16[1,512,2048]{2,1,0:T(8,128)(2,1)} %param.33) | copy-start | bytes 6291460
  6.5 64.4 %copy-start.4 = (f32[4,256]{1,0:T(4,128)S(1)}, f32[4,256]{1,0:T(4,128)}, u32[]{:S(2)}) copy-start(f32[4,256]{1,0:T(4,128)} %param.22) | copy-start | bytes 12292
  6.5 118.4 %reduce-scatter.3.cloned.1.call-start = ((), (), s32[]{:S(2)}) async-start(), calls=%async_computation.4 | async-start | bytes 1310720 | tf_op jit(solution)/shard_map/reduce_scatter | solution.py:101
  86.8 3.5 copy-start.5
  86.8 3.5 copy-start.6
  86.8 38.2 %copy-start.1 = (bf16[64,2048]{1,0:T(8,128)(2,1)S(1)}, bf16[64,2048]{1,0:T(8,128)(2,1)}, u32[]{:S(2)}) copy-start(bf16[64,2048]{1,0:T(8,128)(2,1)} %param.27) | copy-start | bytes 786436
  86.8 39.3 %copy-start.3 = (f32[2048]{0:T(1024)S(1)}, f32[2048]{0:T(1024)}, u32[]{:S(2)}) copy-start(f32[2048]{0:T(1024)} %param.28) | copy-start | bytes 24580
  90.2 147.9 %all-gather.5.cloned.1.call-start = ((), (), s32[]{:S(2)}) async-start(), calls=%async_computation.5 | async-start | bytes 7864320 | tf_op jit(solution)/shard_map/all_gather | solution.py:128
  170.1 158.6 %reduce-scatter.5.cloned.1.call-start = ((), (), s32[]{:S(2)}) async-start(), calls=%async_computation.6 | async-start | bytes 7864320 | tf_op jit(solution)/shard_map/reduce_scatter | solution.py:143
  371.1 1.0 copy-start.2
Sparse Core Ops, SparseCore 0:
  90.4 34.5 reduce-scatter.2
  170.2 67.9 all-gather.4
  258.6 69.9 reduce-scatter.4
where the time goes:
time: 381 us; the launch traced here: 380 us
  waiting for transfers between devices  173 us (45%)
  blocking collectives  143 us (38%)
  matrix products  29.1 us (8%)
  between operations  13.3 us (3%)
  loops' own time  7.86 us (2%)
  other arithmetic  7.23 us (2%)
  local copies, waits for them, and re-layouts  6.88 us (2%)
    reduce_scatter x1, waiting for transfers between devices, local(): lax.psum_scatter(partial_all.astype(jnp.float32).astype(jnp.bfloat16), 't...  70.1 us
    all_gather x1, waiting for transfers between devices, local(): lax.all_gather(lax.all_to_all(outgoing, 'sp', split_axis=0, concat_axis=0...  68.1 us
    all_to_all x1, blocking collectives, local(): lax.all_to_all(summed.astype(jnp.bfloat16), 'sp', split_axis=0, concat_ax...  42.4 us
    all_to_all x1, blocking collectives, local(): lax.all_to_all(outgoing, 'sp', split_axis=0, concat_axis=0, tiled=True)  42.3 us
    reduce_scatter x1, waiting for transfers between devices, local(): lax.psum_scatter(jnp.dot(attended, out_weight, preferred_element_type=jnp...  34.4 us
    all_gather x1, blocking collectives, local(): key_piece = lax.all_gather(key_norm, 'sp', axis=0, tiled=True)  15.8 us
    all_gather x1, blocking collectives, local(): value_piece = lax.all_gather(value_rows, 'sp', axis=0, tiled=True)  15.1 us
    all_gather x1, blocking collectives, local(): lax.all_gather(log_gates, 'sp', axis=1, tiled=True)  14.2 us
  transfers between devices with their start and end apart: 3, of which 3 were waited for; matrix products, arithmetic and copies ran while one was open for 0% of the time, Pallas kernels for 0%

commit v1 on v0

v1 whole, which is shorter than its diff:
```python
import functools

import jax
import jax.numpy as jnp
from jax import lax
from jax.experimental import pallas as pl
from jax.experimental.pallas import tpu as pltpu
from jax.sharding import PartitionSpec as P

EPSILON = 1e-06
CHUNK = 16
MESH = pl.DeviceIdType.MESH


def rms_scale(inputs, gain):
    return inputs * lax.rsqrt(jnp.mean(inputs * inputs, axis=-1, keepdims=True) + EPSILON) * gain


def flip(index, bits):
    index = index + (bits % 2) * (1 - 2 * (index % 2))
    return index + (bits // 2) * (2 - 4 * ((index // 2) % 2))


def greet(nz, n_tp, z, c, t):
    barrier = pltpu.get_barrier_semaphore()
    for dz in range(1, nz):
        pl.semaphore_signal(
            barrier, inc=1, device_id={"sp": 2 * ((z + dz) % nz) + c}, device_id_type=MESH
        )
    for k in range(1, n_tp):
        pl.semaphore_signal(barrier, inc=1, device_id={"tp": flip(t, k)}, device_id_type=MESH)
    pl.semaphore_signal(barrier, inc=1, device_id={"sp": 2 * z + 1 - c}, device_id_type=MESH)
    pl.semaphore_wait(barrier, nz - 1 + n_tp - 1 + 1)


def attend_kernel(
    nz,
    n_tp,
    q_ref,
    kv_ref,
    gd_ref,
    col_ref,
    w_ref,
    res_ref,
    gain_ref,
    mixed_ref,
    normed_ref,
    kv_buf,
    gd_buf,
    m_ref,
    l_ref,
    acc_ref,
    att_ref,
    sbuf,
    rbuf,
    kv_send,
    kv_recv,
    gd_send,
    gd_recv,
    fkv_send,
    fgd_send,
    rs_send,
    rs_recv,
):
    s = lax.axis_index("sp")
    t = lax.axis_index("tp")
    z, c = s // 2, s % 2
    heads, rows, hd = q_ref.shape
    greet(nz, n_tp, z, c, t)

    def own_copies(slot, target):
        return (
            pltpu.make_async_remote_copy(
                kv_ref, kv_buf.at[s], kv_send.at[slot], kv_recv.at[s],
                device_id={"sp": target}, device_id_type=MESH,
            ),
            pltpu.make_async_remote_copy(
                gd_ref, gd_buf.at[s], gd_send.at[slot], gd_recv.at[s],
                device_id={"sp": target}, device_id_type=MESH,
            ),
        )

    def fwd_copies(source, slot):
        return (
            pltpu.make_async_remote_copy(
                kv_buf.at[source], kv_buf.at[source], fkv_send.at[slot], kv_recv.at[source],
                device_id={"sp": 2 * z + 1 - c}, device_id_type=MESH,
            ),
            pltpu.make_async_remote_copy(
                gd_buf.at[source], gd_buf.at[source], fgd_send.at[slot], gd_recv.at[source],
                device_id={"sp": 2 * z + 1 - c}, device_id_type=MESH,
            ),
        )

    def begin(dz, carry):
        for copy in own_copies(dz, 2 * (z + dz) + c):
            copy.start()
        return carry

    @pl.when(c == 0)
    def _():
        for copy in own_copies(0, 2 * z + 1):
            copy.start()

    lax.fori_loop(1, nz - z, begin, 0)

    def update(keys, values, gates, docs, causal, first):
        same = docs == col_ref[:, heads:heads + 1]
        if causal:
            qi = lax.broadcasted_iota(jnp.int32, (rows, rows), 0)
            ki = lax.broadcasted_iota(jnp.int32, (rows, rows), 1)
            same = same & (ki <= qi)
        for h in range(heads):
            scores = lax.dot_general(
                q_ref[h], keys, (((1,), (1,)), ((), ())), preferred_element_type=jnp.float32
            )
            scores = scores + col_ref[:, h:h + 1] - gates[h:h + 1, :]
            scores = jnp.where(same, scores, -jnp.inf)
            peak = jnp.max(scores, axis=-1, keepdims=True)
            if first:
                expo = jnp.exp(scores - peak)
                l_ref[h] = jnp.sum(expo, axis=-1, keepdims=True)
                m_ref[h] = peak
                acc_ref[h] = jnp.dot(
                    expo.astype(jnp.bfloat16), values, preferred_element_type=jnp.float32
                )
            else:
                old = m_ref[h]
                new = jnp.maximum(old, peak)
                expo = jnp.exp(scores - new)
                factor = jnp.exp(old - new)
                l_ref[h] = factor * l_ref[h] + jnp.sum(expo, axis=-1, keepdims=True)
                m_ref[h] = new
                acc_ref[h] = factor * acc_ref[h] + jnp.dot(
                    expo.astype(jnp.bfloat16), values, preferred_element_type=jnp.float32
                )

    update(
        kv_ref[:, :hd], kv_ref[:, hd:], gd_ref[...], gd_ref[heads:heads + 1, :], True, True
    )

    def take(source):
        update(
            kv_buf[source, :, :hd],
            kv_buf[source, :, hd:],
            gd_buf[source],
            gd_buf[source, heads:heads + 1, :],
            False,
            False,
        )

    def one_source(i, carry):
        dz = (i + 1) // 2
        direct = i % 2
        core = (1 - direct) * (1 - c) + direct * c
        source = 2 * (z - dz) + core
        for copy in fwd_copies(source, dz):
            copy.wait_recv()

        @pl.when(direct == 1)
        def _():
            for copy in fwd_copies(source, dz):
                copy.start()

        take(source)
        return carry

    lax.fori_loop(1 - c, 2 * z + 1, one_source, 0)

    for h in range(heads):
        att_ref[:, h * hd:(h + 1) * hd] = (acc_ref[h] / l_ref[h]).astype(jnp.bfloat16)

    share = rows // n_tp

    def project(i, carry):
        k = n_tp - 1 - i
        start = pl.multiple_of(flip(t, k) * share, share)
        block = jnp.dot(
            att_ref[pl.ds(start, share), :], w_ref[...], preferred_element_type=jnp.float32
        )
        sbuf[k] = block.astype(jnp.bfloat16)

        @pl.when(k > 0)
        def _():
            pltpu.make_async_remote_copy(
                sbuf.at[k], rbuf.at[k], rs_send.at[k], rs_recv.at[k],
                device_id={"tp": flip(t, k)}, device_id_type=MESH,
            ).start()

        return carry

    lax.fori_loop(0, n_tp, project, 0)

    for k in range(1, n_tp):
        copy = pltpu.make_async_remote_copy(
            sbuf.at[k], rbuf.at[k], rs_send.at[k], rs_recv.at[k],
            device_id={"tp": flip(t, k)}, device_id_type=MESH,
        )
        copy.wait_recv()

    def finish(i, carry):
        part = pl.ds(pl.multiple_of(i * CHUNK, CHUNK), CHUNK)
        total = sbuf[0, part, :].astype(jnp.float32)
        for k in range(1, n_tp):
            total = total + rbuf[k, part, :].astype(jnp.float32)
        mixed = (res_ref[part, :].astype(jnp.float32) + total).astype(jnp.bfloat16)
        mixed_ref[part, :] = mixed
        normed_ref[part, :] = rms_scale(mixed.astype(jnp.float32), gain_ref[...]).astype(
            jnp.bfloat16
        )
        return carry

    lax.fori_loop(0, share // CHUNK, finish, 0)

    for k in range(1, n_tp):
        pltpu.make_async_remote_copy(
            sbuf.at[k], rbuf.at[k], rs_send.at[k], rs_recv.at[k],
            device_id={"tp": flip(t, k)}, device_id_type=MESH,
        ).wait_send()

    def end(dz, carry):
        for copy in own_copies(dz, 2 * (z + dz) + c):
            copy.wait_send()
        return carry

    @pl.when(c == 0)
    def _():
        for copy in own_copies(0, 2 * z + 1):
            copy.wait_send()

    lax.fori_loop(1, nz - z, end, 0)

    def end_forward(dz, carry):
        for copy in fwd_copies(2 * (z - dz) + c, dz):
            copy.wait_send()
        return carry

    lax.fori_loop(1, z + 1, end_forward, 0)


def expert_kernel(
    nz,
    n_tp,
    out_ref,
    wg_hbm,
    wu_hbm,
    wd_hbm,
    ret_ref,
    wg_ref,
    wu_ref,
    wd_ref,
    arrived,
    part,
    pbuf,
    rbuf,
    hbuf,
    fin,
    w_sem,
    a_send,
    a_recv,
    b_send,
    b_recv,
    f_send,
    f_recv,
    d_send,
    d_recv,
    p_send,
    p_recv,
    h_send,
    h_recv,
    r_send,
    r_recv,
    z_send,
    z_recv,
):
    s = lax.axis_index("sp")
    t = lax.axis_index("tp")
    z, c = s // 2, s % 2
    _, cap, width = out_ref.shape
    rows = nz * cap
    half = nz // 2
    partner = {"sp": 2 * z + 1 - c}

    loads = [
        pltpu.make_async_copy(src, dst, w_sem.at[i])
        for i, (src, dst) in enumerate(((wg_hbm, wg_ref), (wu_hbm, wu_ref), (wd_hbm, wd_ref)))
    ]
    for load in loads:
        load.start()
    greet(nz, n_tp, z, c, t)

    def remote(src, dst, send, recv, where):
        return pltpu.make_async_remote_copy(
            src, dst, send, recv, device_id=where, device_id_type=MESH
        )

    mine = 2 * t + c

    def along(dz):
        target = (z + dz) % nz
        return remote(
            out_ref.at[target], arrived.at[mine, z], a_send.at[dz], a_recv.at[dz],
            {"sp": 2 * target + c},
        )

    def spread(dz, k, src):
        zs = (z + nz - dz) % nz
        return remote(
            src, arrived.at[mine, zs], b_send.at[k, zs], b_recv.at[k, zs], {"tp": flip(t, k)}
        )

    def share_own(dz, src):
        zs = (z + nz - dz) % nz
        return remote(src, arrived.at[mine, zs], b_send.at[0, zs], b_recv.at[0, zs], partner)

    def begin(dz, carry):
        along(dz).start()
        return carry

    for k in (1, 2):
        spread(0, k, out_ref.at[z]).start()
    share_own(0, out_ref.at[z]).start()
    lax.fori_loop(1, nz, begin, 0)
    arrived[mine, z] = out_ref[z]

    def pass_on(dz, carry):
        zs = (z + nz - dz) % nz
        remote(
            out_ref.at[zs], arrived.at[mine, zs], a_send.at[dz], a_recv.at[dz], partner
        ).wait_recv()
        for k in (1, 2):
            spread(dz, k, arrived.at[mine, zs]).start()
        share_own(dz, arrived.at[mine, zs]).start()
        return carry

    lax.fori_loop(1, nz, pass_on, 0)

    def b_wait(k):
        source = 2 * flip(t, k) + c if k else 2 * t + 1 - c

        def one(zs, carry):
            remote(
                arrived.at[source, zs], arrived.at[source, zs], b_send.at[k, zs],
                b_recv.at[k, zs], partner,
            ).wait_recv()
            return carry

        lax.fori_loop(0, nz, one, 0)

    def diagonal(k):
        source = 2 * flip(t, 3 - k) + c
        blocks = pl.ds(0, half) if k == 1 else pl.ds(half, nz - half)
        where = arrived.at[source, blocks]
        return remote(where, where, f_send.at[k], f_recv.at[k], {"tp": flip(t, k)})

    def diagonal_in(k):
        source = 2 * flip(t, 3) + c
        blocks = pl.ds(0, half) if k == 1 else pl.ds(half, nz - half)
        where = arrived.at[source, blocks]
        return remote(where, where, f_send.at[k], f_recv.at[k], {"tp": flip(t, k)})

    def to_partner(k):
        group = arrived.at[2 * flip(t, k) + c]
        return remote(group, group, d_send.at[k], d_recv.at[k], partner)

    def from_partner(k):
        group = arrived.at[2 * flip(t, k) + 1 - c]
        return remote(group, group, d_send.at[k], d_recv.at[k], partner)

    def part_out(k):
        return remote(part.at[1, k], pbuf.at[k], p_send.at[k], p_recv.at[k], partner)

    low, high = pl.ds(0, half), pl.ds(half, nz - half)

    def reduce_out(k, piece):
        blocks = high if piece else low
        return remote(
            part.at[0, k, blocks], rbuf.at[k, blocks], r_send.at[k, piece], r_recv.at[k, piece],
            {"tp": flip(t, k)},
        )

    def hand_over(k):
        blocks = low if k == 1 else high
        return remote(
            part.at[0, 3, blocks], hbuf.at[blocks], h_send.at[k], h_recv.at[k],
            {"tp": flip(t, k)},
        )

    def add_pair(k):
        def one(i, carry):
            b, r = i // (cap // CHUNK), i % (cap // CHUNK)
            at = pl.ds(pl.multiple_of(r * CHUNK, CHUNK), CHUNK)
            total = part[0, k, b, at, :].astype(jnp.float32) + pbuf[k, b, at, :].astype(
                jnp.float32
            )
            part[0, k, b, at, :] = total.astype(jnp.bfloat16)
            return carry

        part_out(k).wait_recv()
        lax.fori_loop(0, rows // CHUNK, one, 0)

    def add_handed(k, first, count):
        def one(i, carry):
            b, r = first + i // (cap // CHUNK), i % (cap // CHUNK)
            at = pl.ds(pl.multiple_of(r * CHUNK, CHUNK), CHUNK)
            total = part[0, k, b, at, :].astype(jnp.float32) + hbuf[b, at, :].astype(jnp.float32)
            part[0, k, b, at, :] = total.astype(jnp.bfloat16)
            return carry

        lax.fori_loop(0, count * (cap // CHUNK), one, 0)

    for load in loads:
        load.wait()

    def compute(i, carry):
        k, other = i // 2, i % 2

        @pl.when(i == 1)
        def _():
            b_wait(0)

        @pl.when(i == 2)
        def _():
            b_wait(1)
            diagonal(2).start()
            to_partner(1).start()
            b_wait(2)
            diagonal(1).start()
            to_partner(2).start()
            add_pair(0)

        @pl.when(i == 3)
        def _():
            from_partner(1).wait_recv()

        @pl.when(i == 4)
        def _():
            add_pair(1)
            reduce_out(1, 0).start()

        @pl.when(i == 5)
        def _():
            from_partner(2).wait_recv()

        @pl.when(i == 6)
        def _():
            add_pair(2)
            reduce_out(2, 1).start()
            diagonal_in(1).wait_recv()
            diagonal_in(2).wait_recv()
            to_partner(3).start()

        @pl.when(i == 7)
        def _():
            from_partner(3).wait_recv()

        column = 2 * flip(t, k) + other * (1 - c) + (1 - other) * c
        flat = arrived[column].reshape(rows, width)
        gate = jnp.dot(flat, wg_ref[...], preferred_element_type=jnp.float32)
        up = jnp.dot(flat, wu_ref[...], preferred_element_type=jnp.float32)
        hidden = (gate * (1.0 / (1.0 + jnp.exp(-gate))) * up).astype(jnp.bfloat16)
        result = jnp.dot(hidden, wd_ref[...], preferred_element_type=jnp.float32)
        part[other, k] = result.astype(jnp.bfloat16).reshape(nz, cap, width)

        for kk in range(n_tp):
            @pl.when(i == 2 * kk + 1)
            def _():
                part_out(kk).start()

        return carry

    lax.fori_loop(0, 2 * n_tp, compute, 0)

    add_pair(3)
    hand_over(1).start()
    hand_over(2).start()
    hand_over(1).wait_recv()
    add_handed(2, 0, half)
    reduce_out(2, 0).start()
    hand_over(2).wait_recv()
    add_handed(1, half, nz - half)
    reduce_out(1, 1).start()

    def home(dz):
        target = (z + dz) % nz
        return remote(
            fin.at[target], ret_ref.at[z], z_send.at[dz], z_recv.at[dz], {"sp": 2 * target + c}
        )

    def total_block(zs, dst, index):
        for r in range(cap // CHUNK):
            at = pl.ds(r * CHUNK, CHUNK)
            total = (
                part[0, 0, zs, at, :].astype(jnp.float32)
                + rbuf[1, zs, at, :].astype(jnp.float32)
                + rbuf[2, zs, at, :].astype(jnp.float32)
            )
            dst[index, at, :] = total.astype(jnp.bfloat16)

    for k in (1, 2):
        for piece in (0, 1):
            reduce_out(k, piece).wait_recv()

    def send_home(i, carry):
        dz = nz - 1 - i
        target = (z + dz) % nz
        total_block(target, fin, target)
        home(dz).start()
        return carry

    lax.fori_loop(0, nz - 1, send_home, 0)
    total_block(z, ret_ref, z)

    def collect(dz, carry):
        zs = (z + nz - dz) % nz
        remote(
            fin.at[zs], ret_ref.at[zs], z_send.at[dz], z_recv.at[dz], partner
        ).wait_recv()
        return carry

    lax.fori_loop(1, nz, collect, 0)

    def drain(dz, carry):
        along(dz).wait_send()
        home(dz).wait_send()
        return carry

    lax.fori_loop(1, nz, drain, 0)

    def drain_spread(dz, carry):
        for k in (1, 2):
            spread(dz, k, out_ref.at[z]).wait_send()
        share_own(dz, out_ref.at[z]).wait_send()
        return carry

    lax.fori_loop(0, nz, drain_spread, 0)
    for k in (1, 2):
        diagonal(k).wait_send()
        hand_over(k).wait_send()
        for piece in (0, 1):
            reduce_out(k, piece).wait_send()
    for k in range(1, n_tp):
        to_partner(k).wait_send()
    for k in range(n_tp):
        part_out(k).wait_send()


def local(
    nz,
    n_tp,
    queries,
    keys,
    values,
    log_gates,
    documents,
    query_gain,
    key_gain,
    out_weight,
    residual,
    norm_gain,
    routes,
    route_weights,
    w_gate,
    w_up,
    w_down,
):
    tok_dev, heads, head_size = queries.shape
    model_dim = residual.shape[1]
    rows_dev = tok_dev // n_tp
    n_sp = 2 * nz
    query_norm = (rms_scale(queries.astype(jnp.float32), query_gain) * head_size ** (-0.5)).astype(
        jnp.bfloat16
    )
    key_norm = rms_scale(keys[:, 0, :].astype(jnp.float32), key_gain).astype(jnp.bfloat16)
    kv = jnp.concatenate([key_norm, values[:, 0, :]], axis=1)
    pad = (-(heads + 1)) % 8
    gates_docs = jnp.concatenate(
        [
            log_gates,
            documents.astype(jnp.float32)[None, :],
            jnp.zeros((pad, tok_dev), jnp.float32),
        ],
        axis=0,
    )
    vmem = pl.BlockSpec(memory_space=pltpu.VMEM)
    hbm = pl.BlockSpec(memory_space=pl.ANY)
    dma = pltpu.SemaphoreType.DMA
    mixed, normed = pl.pallas_call(
        functools.partial(attend_kernel, nz, n_tp),
        out_shape=(
            jax.ShapeDtypeStruct((rows_dev, model_dim), jnp.bfloat16),
            jax.ShapeDtypeStruct((rows_dev, model_dim), jnp.bfloat16),
        ),
        in_specs=[vmem] * 7,
        out_specs=(vmem, vmem),
        scratch_shapes=[
            pltpu.VMEM((n_sp,) + kv.shape, jnp.bfloat16),
            pltpu.VMEM((n_sp,) + gates_docs.shape, jnp.float32),
            pltpu.VMEM((heads, tok_dev, 1), jnp.float32),
            pltpu.VMEM((heads, tok_dev, 1), jnp.float32),
            pltpu.VMEM((heads, tok_dev, head_size), jnp.float32),
            pltpu.VMEM((tok_dev, heads * head_size), jnp.bfloat16),
            pltpu.VMEM((n_tp, rows_dev, model_dim), jnp.bfloat16),
            pltpu.VMEM((n_tp, rows_dev, model_dim), jnp.bfloat16),
            dma((nz,)),
            dma((n_sp,)),
            dma((nz,)),
            dma((n_sp,)),
            dma((nz,)),
            dma((nz,)),
            dma((n_tp,)),
            dma((n_tp,)),
        ],
        compiler_params=pltpu.CompilerParams(
            collective_id=0, has_side_effects=True, vmem_limit_bytes=56 * 1024 * 1024
        ),
        name="attend",
    )(
        jnp.transpose(query_norm, (1, 0, 2)),
        kv,
        gates_docs,
        gates_docs.T,
        out_weight,
        residual,
        norm_gain[None, :],
    )

    experts = nz
    named = min(rows_dev, 6 * rows_dev // n_sp)
    capacity = named + (-named) % CHUNK
    expert_ids = jnp.arange(experts, dtype=jnp.int32)
    chosen = routes[:, :, None] == expert_ids[None, None, :]
    picked = jnp.sum(chosen.astype(jnp.float32), axis=1)
    weight_of = jnp.sum(jnp.where(chosen, route_weights[:, :, None], 0.0), axis=1)
    rank = jnp.cumsum(picked, axis=0) - 1.0
    slot_ids = jnp.arange(capacity).astype(jnp.float32)
    placing = picked.T[:, None, :] * (rank.T[:, None, :] == slot_ids[None, :, None]).astype(
        jnp.float32
    )
    outgoing = jnp.einsum(
        "ecr,rd->ecd", placing.astype(jnp.bfloat16), normed, preferred_element_type=jnp.float32
    ).astype(jnp.bfloat16)

    hidden_dev = w_gate.shape[2]
    block = (nz, capacity, model_dim)
    returned = pl.pallas_call(
        functools.partial(expert_kernel, nz, n_tp),
        out_shape=jax.ShapeDtypeStruct(block, jnp.bfloat16),
        in_specs=[vmem, hbm, hbm, hbm],
        out_specs=vmem,
        scratch_shapes=[
            pltpu.VMEM((model_dim, hidden_dev), jnp.bfloat16),
            pltpu.VMEM((model_dim, hidden_dev), jnp.bfloat16),
            pltpu.VMEM((hidden_dev, model_dim), jnp.bfloat16),
            pltpu.VMEM((2 * n_tp,) + block, jnp.bfloat16),
            pltpu.VMEM((2, n_tp) + block, jnp.bfloat16),
            pltpu.VMEM((n_tp,) + block, jnp.bfloat16),
            pltpu.VMEM((3,) + block, jnp.bfloat16),
            pltpu.VMEM(block, jnp.bfloat16),
            pltpu.VMEM(block, jnp.bfloat16),
            dma((3,)),
            dma((nz,)),
            dma((nz,)),
            dma((3, nz)),
            dma((3, nz)),
            dma((3,)),
            dma((3,)),
            dma((n_tp,)),
            dma((n_tp,)),
            dma((n_tp,)),
            dma((n_tp,)),
            dma((3,)),
            dma((3,)),
            dma((3, 2)),
            dma((3, 2)),
            dma((nz,)),
            dma((nz,)),
        ],
        compiler_params=pltpu.CompilerParams(
            collective_id=1, has_side_effects=True, vmem_limit_bytes=60 * 1024 * 1024
        ),
        name="experts",
    )(outgoing, w_gate[0], w_up[0], w_down[0])

    combining = placing * weight_of.T[:, None, :]
    routed = jnp.einsum(
        "ecr,ecd->rd", combining, returned.astype(jnp.float32), precision=lax.Precision.HIGHEST
    )
    return (mixed.astype(jnp.float32) + routed).astype(jnp.bfloat16)


def solution(mesh):
    return jax.shard_map(
        functools.partial(local, mesh.shape["sp"] // 2, mesh.shape["tp"]),
        mesh=mesh,
        in_specs=(
            P(("grp", "sp"), "tp", None),
            P(("grp", "sp"), "tp", None),
            P(("grp", "sp"), "tp", None),
            P("tp", ("grp", "sp")),
            P(("grp", "sp")),
            P(),
            P(),
            P("tp", None),
            P(("grp", "sp", "tp"), None),
            P(),
            P(("grp", "sp", "tp"), None),
            P(("grp", "sp", "tp"), None),
            P("sp", None, "tp"),
            P("sp", None, "tp"),
            P("sp", "tp", None),
        ),
        out_specs=P(("grp", "sp", "tp"), None),
        check_vma=False,
    )
```

time: 381 us -> 151 us (0.40)
  waiting for transfers between devices: 173 us -> 0 us
  blocking collectives: 143 us -> 0 us
  Pallas kernels: 0 us -> 136 us
  matrix products: 29.1 us -> 4.74 us
  between operations: 13.3 us -> 0.06 us
  loops' own time: 7.86 us -> 0 us
  local copies, waits for them, and re-layouts: 6.88 us -> 1.04 us
    pallas_call x0 -> x2, Pallas kernels: none -> 136 us  [the longest x1 110 us: local(): pl.pallas_call(functools.partial(expert_kernel, nz, n_tp), out_shape=jax....]
    reduce_scatter x2 -> x0, waiting for transfers between devices: 105 us -> none  [the longest x1 70.1 us: local(): lax.psum_scatter(partial_all.astype(jnp.float32).astype(jnp.bfloat16), 't...]
    all_to_all x2 -> x0, blocking collectives: 84.7 us -> none  [the longest x1 42.4 us: local(): lax.all_to_all(summed.astype(jnp.bfloat16), 'sp', split_axis=0, concat_ax...]
    all_gather x1 -> x0, waiting for transfers between devices: 68.1 us -> none  [local(): lax.all_gather(lax.all_to_all(outgoing, 'sp', split_axis=0, concat_axis=0...]
    all_gather x4 -> x0, blocking collectives: 58.6 us -> none  [the longest x1 15.8 us: local(): key_piece = lax.all_gather(key_norm, 'sp', axis=0, tiled=True)]
    dot_general x6 -> x1, matrix products: 27.7 us -> 2.5 us  [local(): jnp.einsum('ecr,ecd->rd', combining, returned.astype(jnp.float32), precis...]
    another operation x5 -> x0, loops' own time: 7.86 us -> none  [the longest x1 7.74 us: local(): lax.scan(one_block, start_state, jnp.arange(block_count, dtype=jnp.int32))]
  transfers between devices with their start and end apart: 3 -> 0, of which waited for: 3 -> 0; matrix products, arithmetic and copies ran while one was open for 0% -> 0% of each run, Pallas kernels for 0% -> 0%
where the time goes in v1:
time: 151 us; the launch traced here: 150 us
  Pallas kernels  136 us (90%)
  other arithmetic  8.71 us (6%)
  matrix products  4.74 us (3%)
    pallas_call x1, Pallas kernels, local(): pl.pallas_call(functools.partial(expert_kernel, nz, n_tp), out_shape=jax....  110 us
    pallas_call x1, Pallas kernels, local(): pl.pallas_call(functools.partial(attend_kernel, nz, n_tp), out_shape=(jax...  25.1 us

profile of v1, /device:TPU:0, one launch (start us, length us, event | category | flops | bytes accessed | tf_op | source)
XLA Modules:
  0.0 150.1 jit_solution(12959640031493661796)
XLA Ops:
  0.0 0.1 pad.2.clone
  0.1 0.7 convert_element_type.47
  0.8 0.9 fusion.8
  1.7 1.2 fusion.2
  2.9 0.7 select_reduce_fusion
  3.6 0.8 maximum_maximum_fusion.gd_ref
  4.4 0.0 copy-start.1
  4.4 0.1 copy.39
  4.5 0.1 reduce_window_sum.11
  4.6 0.1 copy.40
  4.7 1.0 fusion.10
  5.6 1.5 %pad_maximum_fusion.kv_ref = bf16[256,256]{1,0:T(8,128)(2,1)} fusion(bf16[256,128]{1,0:T(8,128)(2,1)} %bitcast.31, bf16[256,128]{1,0:T(8,128)(2,1)S(1)} %fusion.10), kind=kLoop, calls=%fused_computation.17 | loop fusion | flops 262144 | bytes 262144 | tf_op jit(solution)/shard_map/concatenate | solution.py:575
  7.1 0.8 copy.38
  7.9 1.9 %fusion.6.q_ref = bf16[4,256,128]{2,1,0:T(8,128)(2,1)} fusion(f32[128]{0:T(128)} %param.20, f32[256,4]{0,1:T(4,128)S(1)} %add_rsqrt_fusion, bf16[256,4,128]{2,1,0:T(4,128)(2,1)} %param.15), kind=kLoop, calls=%fused_computation.10 | loop fusion | flops 655360 | bytes 528896 | tf_op jit(solution)/shard_map/transpose | solution.py:619
  9.8 0.0 copy-done.1
  9.8 25.1 %attend.1 = (bf16[64,2048]{1,0:T(8,128)(2,1)}, bf16[64,2048]{1,0:T(8,128)(2,1)}) custom-call(bf16[4,256,128]{2,1,0:T(8,128)(2,1)} %fusion.6.q_ref, bf16[256,256]{1,0:T(8,128)(2,1)} %pad_maximum_fusion.kv_ref, f32[8,256]{1,0:T(8,128)} %copy-done.1, f32[256,8]{1,0:T(8,128)} %bitcast.30, bf16[512,2048]{1,0:T(8,128)(2,1)} %w_ref.1, bf16[64,2048]{1,0:T(8,128)(2,1)} %res_ref.1, ...), custom_call_target="tpu_custom_call" | custom-call | tf_op jit(solution)/shard_map/attend/pallas_call | solution.py:588
  34.9 2.2 %convolution_convert_fusion.out_ref = bf16[4,48,2048]{2,1,0:T(8,128)(2,1)} fusion(bf16[64,2048]{1,0:T(8,128)(2,1)} %get-tuple-element.8, f32[4,64]{1,0:T(4,128)S(1)} %bitcast.32, f32[4,64]{1,0:T(4,128)S(1)} %copy.40, f32[48]{0:T(128)S(1)} %iota_convert_fusion), kind=kOutput, calls=%fused_computation | convolution fusion | flops 50749440 | bytes 1050816 | tf_op jit(solution)/shard_map/ecr,rd->ecd/dot_general | solution.py:640
  37.1 0.0 copy-start
  37.1 110.5 %experts.1 = bf16[4,48,2048]{2,1,0:T(8,128)(2,1)} custom-call(bf16[4,48,2048]{2,1,0:T(8,128)(2,1)} %convolution_convert_fusion.out_ref, bf16[2048,512]{1,0:T(8,128)(2,1)} %bitcast.27, bf16[2048,512]{1,0:T(8,128)(2,1)} %bitcast.28, bf16[512,2048]{1,0:T(8,128)(2,1)} %bitcast.29), custom_call_target="tpu_custom_call" | custom-call | tf_op jit(solution)/shard_map/experts/pallas_call | solution.py:646
  147.6 0.0 copy-done
  147.6 2.5 %fusion.1 = bf16[64,2048]{1,0:T(8,128)(2,1)} fusion(bf16[4,48,2048]{2,1,0:T(8,128)(2,1)} %experts.1, bf16[64,2048]{1,0:T(8,128)(2,1)S(1)} %copy-done, f32[4,64]{1,0:T(4,128)S(1)} %bitcast.35, f32[4,64]{1,0:T(4,128)S(1)} %bitcast.33, f32[4,64]{1,0:T(4,128)S(1)} %copy.40, f32[48]{0:T(128)S(1)} %iota_convert_fusion), kind=kOutput, calls=%fused_computation.3 | convolution fusion | flops 302419968 | bytes 1313984 | tf_op jit(solution)/shard_map/ecr,ecd->rd/dot_general | solution.py:686
  (5 shorter events, 0.0 us)
Async XLA Ops:
  4.4 5.4 %copy-start.1 = (f32[8,256]{1,0:T(8,128)}, f32[8,256]{1,0:T(8,128)S(1)}, u32[]{:S(2)}) copy-start(f32[8,256]{1,0:T(8,128)S(1)} %maximum_maximum_fusion.gd_ref) | copy-start | bytes 24580
  37.1 110.5 %copy-start = (bf16[64,2048]{1,0:T(8,128)(2,1)S(1)}, bf16[64,2048]{1,0:T(8,128)(2,1)}, u32[]{:S(2)}) copy-start(bf16[64,2048]{1,0:T(8,128)(2,1)} %get-tuple-element.7) | copy-start | bytes 786436

commit v2 on v1

--- a/solution.py
+++ b/solution.py
@@ -277,9 +277,10 @@
     t = lax.axis_index("tp")
     z, c = s // 2, s % 2
     _, cap, width = out_ref.shape
-    rows = nz * cap
-    half = nz // 2
+    rows = 2 * n_tp * cap
     partner = {"sp": 2 * z + 1 - c}
+    near = 1 + c
+    far = 2 - c
 
     loads = [
         pltpu.make_async_copy(src, dst, w_sem.at[i])
@@ -294,255 +295,215 @@
             src, dst, send, recv, device_id=where, device_id_type=MESH
         )
 
-    mine = 2 * t + c
-
-    def along(dz):
-        target = (z + dz) % nz
+    def source_of(q):
+        return (z + nz - q) % nz
+
+    def mine(q):
+        return arrived.at[source_of(q), c, t]
+
+    def along(q):
+        target = (z + q) % nz
         return remote(
-            out_ref.at[target], arrived.at[mine, z], a_send.at[dz], a_recv.at[dz],
+            out_ref.at[target], arrived.at[z, c, t], a_send.at[q], a_recv.at[q],
             {"sp": 2 * target + c},
         )
 
-    def spread(dz, k, src):
-        zs = (z + nz - dz) % nz
+    def along_in(q):
+        return remote(mine(q), mine(q), a_send.at[q], a_recv.at[q], partner)
+
+    def spread(q, k, src):
+        where = {"tp": flip(t, k)} if k else partner
+        return remote(src, mine(q), b_send.at[k, q], b_recv.at[k, q], where)
+
+    def spread_in(q, k):
+        block = arrived.at[source_of(q), c, flip(t, k)] if k else arrived.at[
+            source_of(q), 1 - c, t
+        ]
+        return remote(block, block, b_send.at[k, q], b_recv.at[k, q], partner)
+
+    def diagonal(q):
+        block = arrived.at[source_of(q), c, flip(t, far)]
+        return remote(block, block, f_send.at[q], f_recv.at[q], {"tp": flip(t, near)})
+
+    def diagonal_in(q):
+        block = arrived.at[source_of(q), c, flip(t, 3)]
+        return remote(block, block, f_send.at[q], f_recv.at[q], partner)
+
+    def to_partner(q, k):
+        block = arrived.at[source_of(q), c, flip(t, k)]
+        return remote(block, block, d_send.at[k, q], d_recv.at[k, q], partner)
+
+    def from_partner(q, k):
+        block = arrived.at[source_of(q), 1 - c, flip(t, k)]
+        return remote(block, block, d_send.at[k, q], d_recv.at[k, q], partner)
+
+    def part_out(q):
+        return remote(part.at[q, 1 - c], pbuf.at[q], p_send.at[q], p_recv.at[q], partner)
+
+    def hand_over(q):
         return remote(
-            src, arrived.at[mine, zs], b_send.at[k, zs], b_recv.at[k, zs], {"tp": flip(t, k)}
-        )
-
-    def share_own(dz, src):
-        zs = (z + nz - dz) % nz
-        return remote(src, arrived.at[mine, zs], b_send.at[0, zs], b_recv.at[0, zs], partner)
-
-    def begin(dz, carry):
-        along(dz).start()
-        return carry
-
-    for k in (1, 2):
+            part.at[q, c, flip(t, 3)], hbuf.at[q], h_send.at[q], h_recv.at[q],
+            {"tp": flip(t, near)},
+        )
+
+    def reduce_near(q):
+        return remote(
+            part.at[q, c, flip(t, near)], rbuf.at[q, 0], r_send.at[0, q], r_recv.at[0, q],
+            {"tp": flip(t, near)},
+        )
+
+    def reduce_far(q):
+        return remote(
+            part.at[q, c, flip(t, far)], rbuf.at[q, 1], r_send.at[1, q], r_recv.at[1, q],
+            {"tp": flip(t, far)},
+        )
+
+    def home(q):
+        return remote(
+            fin.at[q], ret_ref.at[z], z_send.at[q], z_recv.at[q], {"sp": 2 * source_of(q) + c}
+        )
+
+    def home_in(q):
+        return remote(
+            fin.at[q], ret_ref.at[(z + q) % nz], z_send.at[q], z_recv.at[q], partner
+        )
+
+    for k in (1, 2, 0):
         spread(0, k, out_ref.at[z]).start()
-    share_own(0, out_ref.at[z]).start()
+
+    def begin(q, carry):
+        along(q).start()
+        return carry
+
     lax.fori_loop(1, nz, begin, 0)
-    arrived[mine, z] = out_ref[z]
-
-    def pass_on(dz, carry):
-        zs = (z + nz - dz) % nz
-        remote(
-            out_ref.at[zs], arrived.at[mine, zs], a_send.at[dz], a_recv.at[dz], partner
-        ).wait_recv()
-        for k in (1, 2):
-            spread(dz, k, arrived.at[mine, zs]).start()
-        share_own(dz, arrived.at[mine, zs]).start()
-        return carry
-
-    lax.fori_loop(1, nz, pass_on, 0)
-
-    def b_wait(k):
-        source = 2 * flip(t, k) + c if k else 2 * t + 1 - c
-
-        def one(zs, carry):
-            remote(
-                arrived.at[source, zs], arrived.at[source, zs], b_send.at[k, zs],
-                b_recv.at[k, zs], partner,
-            ).wait_recv()
-            return carry
-
-        lax.fori_loop(0, nz, one, 0)
-
-    def diagonal(k):
-        source = 2 * flip(t, 3 - k) + c
-        blocks = pl.ds(0, half) if k == 1 else pl.ds(half, nz - half)
-        where = arrived.at[source, blocks]
-        return remote(where, where, f_send.at[k], f_recv.at[k], {"tp": flip(t, k)})
-
-    def diagonal_in(k):
-        source = 2 * flip(t, 3) + c
-        blocks = pl.ds(0, half) if k == 1 else pl.ds(half, nz - half)
-        where = arrived.at[source, blocks]
-        return remote(where, where, f_send.at[k], f_recv.at[k], {"tp": flip(t, k)})
-
-    def to_partner(k):
-        group = arrived.at[2 * flip(t, k) + c]
-        return remote(group, group, d_send.at[k], d_recv.at[k], partner)
-
-    def from_partner(k):
-        group = arrived.at[2 * flip(t, k) + 1 - c]
-        return remote(group, group, d_send.at[k], d_recv.at[k], partner)
-
-    def part_out(k):
-        return remote(part.at[1, k], pbuf.at[k], p_send.at[k], p_recv.at[k], partner)
-
-    low, high = pl.ds(0, half), pl.ds(half, nz - half)
-
-    def reduce_out(k, piece):
-        blocks = high if piece else low
-        return remote(
-            part.at[0, k, blocks], rbuf.at[k, blocks], r_send.at[k, piece], r_recv.at[k, piece],
-            {"tp": flip(t, k)},
-        )
-
-    def hand_over(k):
-        blocks = low if k == 1 else high
-        return remote(
-            part.at[0, 3, blocks], hbuf.at[blocks], h_send.at[k], h_recv.at[k],
-            {"tp": flip(t, k)},
-        )
-
-    def add_pair(k):
-        def one(i, carry):
-            b, r = i // (cap // CHUNK), i % (cap // CHUNK)
-            at = pl.ds(pl.multiple_of(r * CHUNK, CHUNK), CHUNK)
-            total = part[0, k, b, at, :].astype(jnp.float32) + pbuf[k, b, at, :].astype(
-                jnp.float32
-            )
-            part[0, k, b, at, :] = total.astype(jnp.bfloat16)
-            return carry
-
-        part_out(k).wait_recv()
-        lax.fori_loop(0, rows // CHUNK, one, 0)
-
-    def add_handed(k, first, count):
-        def one(i, carry):
-            b, r = first + i // (cap // CHUNK), i % (cap // CHUNK)
-            at = pl.ds(pl.multiple_of(r * CHUNK, CHUNK), CHUNK)
-            total = part[0, k, b, at, :].astype(jnp.float32) + hbuf[b, at, :].astype(jnp.float32)
-            part[0, k, b, at, :] = total.astype(jnp.bfloat16)
-            return carry
-
-        lax.fori_loop(0, count * (cap // CHUNK), one, 0)
-
+    arrived[z, c, t] = out_ref[z]
     for load in loads:
         load.wait()
 
-    def compute(i, carry):
-        k, other = i // 2, i % 2
-
-        @pl.when(i == 1)
-        def _():
-            b_wait(0)
-
-        @pl.when(i == 2)
-        def _():
-            b_wait(1)
-            diagonal(2).start()
-            to_partner(1).start()
-            b_wait(2)
-            diagonal(1).start()
-            to_partner(2).start()
-            add_pair(0)
-
-        @pl.when(i == 3)
-        def _():
-            from_partner(1).wait_recv()
-
-        @pl.when(i == 4)
-        def _():
-            add_pair(1)
-            reduce_out(1, 0).start()
-
-        @pl.when(i == 5)
-        def _():
-            from_partner(2).wait_recv()
-
-        @pl.when(i == 6)
-        def _():
-            add_pair(2)
-            reduce_out(2, 1).start()
-            diagonal_in(1).wait_recv()
-            diagonal_in(2).wait_recv()
-            to_partner(3).start()
-
-        @pl.when(i == 7)
-        def _():
-            from_partner(3).wait_recv()
-
-        column = 2 * flip(t, k) + other * (1 - c) + (1 - other) * c
-        flat = arrived[column].reshape(rows, width)
-        gate = jnp.dot(flat, wg_ref[...], preferred_element_type=jnp.float32)
-        up = jnp.dot(flat, wu_ref[...], preferred_element_type=jnp.float32)
-        hidden = (gate * (1.0 / (1.0 + jnp.exp(-gate))) * up).astype(jnp.bfloat16)
-        result = jnp.dot(hidden, wd_ref[...], preferred_element_type=jnp.float32)
-        part[other, k] = result.astype(jnp.bfloat16).reshape(nz, cap, width)
-
-        for kk in range(n_tp):
-            @pl.when(i == 2 * kk + 1)
+    def add_pair(q, column):
+        def one(r, carry):
+            at = pl.ds(pl.multiple_of(r * CHUNK, CHUNK), CHUNK)
+            total = part[q, c, column, at, :].astype(jnp.float32) + pbuf[
+                q, column, at, :
+            ].astype(jnp.float32)
+            part[q, c, column, at, :] = total.astype(jnp.bfloat16)
+            return carry
+
+        lax.fori_loop(0, cap // CHUNK, one, 0)
+
+    def step(i, carry):
+        p = i - 1
+
+        @pl.when(p + 2 < nz)
+        def _():
+            q = p + 2
+            along_in(q).wait_recv()
+            for k in (1, 2, 0):
+                spread(q, k, mine(q)).start()
+
+        @pl.when(p + 1 < nz)
+        def _():
+            q = p + 1
+            spread_in(q, 1).wait_recv()
+            to_partner(q, 1).start()
+            spread_in(q, 2).wait_recv()
+            diagonal(q).start()
+            to_partner(q, 2).start()
+            spread_in(q, 0).wait_recv()
+
+        @pl.when((p >= 0) & (p < nz))
+        def _():
+            diagonal_in(p).wait_recv()
+            to_partner(p, 3).start()
+            for k in range(1, n_tp):
+                from_partner(p, k).wait_recv()
+            flat = arrived[source_of(p)].reshape(rows, width)
+            gate = jnp.dot(flat, wg_ref[...], preferred_element_type=jnp.float32)
+            up = jnp.dot(flat, wu_ref[...], preferred_element_type=jnp.float32)
+            hidden = (gate * (1.0 / (1.0 + jnp.exp(-gate))) * up).astype(jnp.bfloat16)
+            result = jnp.dot(hidden, wd_ref[...], preferred_element_type=jnp.float32)
+            part[p] = result.astype(jnp.bfloat16).reshape(2, n_tp, cap, width)
+            part_out(p).start()
+
+        @pl.when((p >= 1) & (p - 1 < nz))
+        def _():
+            q = p - 1
+            part_out(q).wait_recv()
+            add_pair(q, flip(t, 3))
+            hand_over(q).start()
+            add_pair(q, flip(t, near))
+            reduce_near(q).start()
+            add_pair(q, flip(t, far))
+            add_pair(q, t)
+
+        @pl.when((p >= 2) & (p - 2 < nz))
+        def _():
+            q = p - 2
+            column = flip(t, far)
+            hand_over(q).wait_recv()
+
+            def one(r, carry):
+                at = pl.ds(pl.multiple_of(r * CHUNK, CHUNK), CHUNK)
+                total = part[q, c, column, at, :].astype(jnp.float32) + hbuf[q, at, :].astype(
+                    jnp.float32
+                )
+                part[q, c, column, at, :] = total.astype(jnp.bfloat16)
+                return carry
+
+            lax.fori_loop(0, cap // CHUNK, one, 0)
+            reduce_far(q).start()
+
+        @pl.when(p >= 3)
+        def _():
+            q = p - 3
+            reduce_near(q).wait_recv()
+            reduce_far(q).wait_recv()
+
+            def one(r, carry):
+                at = pl.ds(pl.multiple_of(r * CHUNK, CHUNK), CHUNK)
+                total = (
+                    part[q, c, t, at, :].astype(jnp.float32)
+                    + rbuf[q, 0, at, :].astype(jnp.float32)
+                    + rbuf[q, 1, at, :].astype(jnp.float32)
+                )
+                fin[q, at, :] = total.astype(jnp.bfloat16)
+                return carry
+
+            lax.fori_loop(0, cap // CHUNK, one, 0)
+
+            @pl.when(q > 0)
             def _():
-                part_out(kk).start()
-
-        return carry
-
-    lax.fori_loop(0, 2 * n_tp, compute, 0)
-
-    add_pair(3)
-    hand_over(1).start()
-    hand_over(2).start()
-    hand_over(1).wait_recv()
-    add_handed(2, 0, half)
-    reduce_out(2, 0).start()
-    hand_over(2).wait_recv()
-    add_handed(1, half, nz - half)
-    reduce_out(1, 1).start()
-
-    def home(dz):
-        target = (z + dz) % nz
-        return remote(
-            fin.at[target], ret_ref.at[z], z_send.at[dz], z_recv.at[dz], {"sp": 2 * target + c}
-        )
-
-    def total_block(zs, dst, index):
-        for r in range(cap // CHUNK):
-            at = pl.ds(r * CHUNK, CHUNK)
-            total = (
-                part[0, 0, zs, at, :].astype(jnp.float32)
-                + rbuf[1, zs, at, :].astype(jnp.float32)
-                + rbuf[2, zs, at, :].astype(jnp.float32)
-            )
-            dst[index, at, :] = total.astype(jnp.bfloat16)
-
-    for k in (1, 2):
-        for piece in (0, 1):
-            reduce_out(k, piece).wait_recv()
-
-    def send_home(i, carry):
-        dz = nz - 1 - i
-        target = (z + dz) % nz
-        total_block(target, fin, target)
-        home(dz).start()
-        return carry
-
-    lax.fori_loop(0, nz - 1, send_home, 0)
-    total_block(z, ret_ref, z)
-
-    def collect(dz, carry):
-        zs = (z + nz - dz) % nz
-        remote(
-            fin.at[zs], ret_ref.at[zs], z_send.at[dz], z_recv.at[dz], partner
-        ).wait_recv()
-        return carry
-
-    lax.fori_loop(1, nz, collect, 0)
-
-    def drain(dz, carry):
-        along(dz).wait_send()
-        home(dz).wait_send()
+                home(q).start()
+
+            @pl.when(q == 0)
+            def _():
+                ret_ref[z] = fin[0]
+
+        return carry
+
+    lax.fori_loop(0, nz + 4, step, 0)
+
+    def drain(q, carry):
+        home_in(q).wait_recv()
+        home(q).wait_send()
+        along(q).wait_send()
         return carry
 
     lax.fori_loop(1, nz, drain, 0)
 
-    def drain_spread(dz, carry):
-        for k in (1, 2):
-            spread(dz, k, out_ref.at[z]).wait_send()
-        share_own(dz, out_ref.at[z]).wait_send()
-        return carry
-
-    lax.fori_loop(0, nz, drain_spread, 0)
-    for k in (1, 2):
-        diagonal(k).wait_send()
-        hand_over(k).wait_send()
-        for piece in (0, 1):
-            reduce_out(k, piece).wait_send()
-    for k in range(1, n_tp):
-        to_partner(k).wait_send()
-    for k in range(n_tp):
-        part_out(k).wait_send()
+    def drain_plane(q, carry):
+        for k in range(3):
+            spread(q, k, mine(q)).wait_send()
+        diagonal(q).wait_send()
+        for k in range(1, n_tp):
+            to_partner(q, k).wait_send()
+        part_out(q).wait_send()
+        hand_over(q).wait_send()
+        reduce_near(q).wait_send()
+        reduce_far(q).wait_send()
+        return carry
+
+    lax.fori_loop(0, nz, drain_plane, 0)
 
 
 def local(
@@ -652,10 +613,10 @@
             pltpu.VMEM((model_dim, hidden_dev), jnp.bfloat16),
             pltpu.VMEM((model_dim, hidden_dev), jnp.bfloat16),
             pltpu.VMEM((hidden_dev, model_dim), jnp.bfloat16),
-            pltpu.VMEM((2 * n_tp,) + block, jnp.bfloat16),
-            pltpu.VMEM((2, n_tp) + block, jnp.bfloat16),
-            pltpu.VMEM((n_tp,) + block, jnp.bfloat16),
-            pltpu.VMEM((3,) + block, jnp.bfloat16),
+            pltpu.VMEM((nz, 2, n_tp) + block[1:], jnp.bfloat16),
+            pltpu.VMEM((nz, 2, n_tp) + block[1:], jnp.bfloat16),
+            pltpu.VMEM((nz, n_tp) + block[1:], jnp.bfloat16),
+            pltpu.VMEM((nz, 2) + block[1:], jnp.bfloat16),
             pltpu.VMEM(block, jnp.bfloat16),
             pltpu.VMEM(block, jnp.bfloat16),
             dma((3,)),
@@ -663,16 +624,16 @@
             dma((nz,)),
             dma((3, nz)),
             dma((3, nz)),
-            dma((3,)),
-            dma((3,)),
-            dma((n_tp,)),
-            dma((n_tp,)),
-            dma((n_tp,)),
-            dma((n_tp,)),
-            dma((3,)),
-            dma((3,)),
-            dma((3, 2)),
-            dma((3, 2)),
+            dma((nz,)),
+            dma((nz,)),
+            dma((n_tp, nz)),
+            dma((n_tp, nz)),
+            dma((nz,)),
+            dma((nz,)),
+            dma((nz,)),
+            dma((nz,)),
+            dma((2, nz)),
+            dma((2, nz)),
             dma((nz,)),
             dma((nz,)),
         ],

time: 151 us -> 137 us (0.907)
  Pallas kernels: 136 us -> 122 us
    pallas_call x1, Pallas kernels: 110 us -> 97 us  [local(): pl.pallas_call(functools.partial(expert_kernel, nz, n_tp), out_shape=jax....]
where the time goes in v2:
time: 137 us
  Pallas kernels  122 us (89%)
  other arithmetic  8.71 us (6%)
  matrix products  4.74 us (3%)
    pallas_call x1, Pallas kernels, local(): pl.pallas_call(functools.partial(expert_kernel, nz, n_tp), out_shape=jax....  97 us
    pallas_call x1, Pallas kernels, local(): pl.pallas_call(functools.partial(attend_kernel, nz, n_tp), out_shape=(jax...  25.1 us

profile of v2, /device:TPU:0, one launch (start us, length us, event | category | flops | bytes accessed | tf_op | source)
XLA Modules:
  0.0 136.7 jit_solution(2993767806608110975)
XLA Ops:
  0.0 0.1 pad.2.clone
  0.1 0.7 convert_element_type.47
  0.8 0.9 fusion.8
  1.7 1.2 fusion.2
  2.9 0.7 select_reduce_fusion
  3.6 0.8 maximum_maximum_fusion.gd_ref
  4.4 0.0 copy-start.1
  4.4 0.1 copy.39
  4.5 0.1 reduce_window_sum.11
  4.6 0.1 copy.40
  4.7 1.0 fusion.10
  5.6 1.5 %pad_maximum_fusion.kv_ref = bf16[256,256]{1,0:T(8,128)(2,1)} fusion(bf16[256,128]{1,0:T(8,128)(2,1)} %bitcast.31, bf16[256,128]{1,0:T(8,128)(2,1)S(1)} %fusion.10), kind=kLoop, calls=%fused_computation.17 | loop fusion | flops 262144 | bytes 262144 | tf_op jit(solution)/shard_map/concatenate | solution.py:536
  7.1 0.8 copy.38
  7.9 1.9 %fusion.6.q_ref = bf16[4,256,128]{2,1,0:T(8,128)(2,1)} fusion(f32[128]{0:T(128)} %param.20, f32[256,4]{0,1:T(4,128)S(1)} %add_rsqrt_fusion, bf16[256,4,128]{2,1,0:T(4,128)(2,1)} %param.15), kind=kLoop, calls=%fused_computation.10 | loop fusion | flops 655360 | bytes 528896 | tf_op jit(solution)/shard_map/transpose | solution.py:580
  9.8 0.0 copy-done.1
  9.8 25.1 %attend.1 = (bf16[64,2048]{1,0:T(8,128)(2,1)}, bf16[64,2048]{1,0:T(8,128)(2,1)}) custom-call(bf16[4,256,128]{2,1,0:T(8,128)(2,1)} %fusion.6.q_ref, bf16[256,256]{1,0:T(8,128)(2,1)} %pad_maximum_fusion.kv_ref, f32[8,256]{1,0:T(8,128)} %copy-done.1, f32[256,8]{1,0:T(8,128)} %bitcast.30, bf16[512,2048]{1,0:T(8,128)(2,1)} %w_ref.1, bf16[64,2048]{1,0:T(8,128)(2,1)} %res_ref.1, ...), custom_call_target="tpu_custom_call" | custom-call | tf_op jit(solution)/shard_map/attend/pallas_call | solution.py:549
  34.9 2.2 %convolution_convert_fusion.out_ref = bf16[4,48,2048]{2,1,0:T(8,128)(2,1)} fusion(bf16[64,2048]{1,0:T(8,128)(2,1)} %get-tuple-element.8, f32[4,64]{1,0:T(4,128)S(1)} %bitcast.32, f32[4,64]{1,0:T(4,128)S(1)} %copy.40, f32[48]{0:T(128)S(1)} %iota_convert_fusion), kind=kOutput, calls=%fused_computation | convolution fusion | flops 50749440 | bytes 1050816 | tf_op jit(solution)/shard_map/ecr,rd->ecd/dot_general | solution.py:601
  37.1 0.0 copy-start
  37.1 97.0 %experts.1 = bf16[4,48,2048]{2,1,0:T(8,128)(2,1)} custom-call(bf16[4,48,2048]{2,1,0:T(8,128)(2,1)} %convolution_convert_fusion.out_ref, bf16[2048,512]{1,0:T(8,128)(2,1)} %bitcast.27, bf16[2048,512]{1,0:T(8,128)(2,1)} %bitcast.28, bf16[512,2048]{1,0:T(8,128)(2,1)} %bitcast.29), custom_call_target="tpu_custom_call" | custom-call | tf_op jit(solution)/shard_map/experts/pallas_call | solution.py:607
  134.2 0.0 copy-done
  134.2 2.5 %fusion.1 = bf16[64,2048]{1,0:T(8,128)(2,1)} fusion(bf16[4,48,2048]{2,1,0:T(8,128)(2,1)} %experts.1, bf16[64,2048]{1,0:T(8,128)(2,1)S(1)} %copy-done, f32[4,64]{1,0:T(4,128)S(1)} %bitcast.35, f32[4,64]{1,0:T(4,128)S(1)} %bitcast.33, f32[4,64]{1,0:T(4,128)S(1)} %copy.40, f32[48]{0:T(128)S(1)} %iota_convert_fusion), kind=kOutput, calls=%fused_computation.3 | convolution fusion | flops 302419968 | bytes 1313984 | tf_op jit(solution)/shard_map/ecr,ecd->rd/dot_general | solution.py:647
  (5 shorter events, 0.0 us)
Async XLA Ops:
  4.4 5.4 %copy-start.1 = (f32[8,256]{1,0:T(8,128)}, f32[8,256]{1,0:T(8,128)S(1)}, u32[]{:S(2)}) copy-start(f32[8,256]{1,0:T(8,128)S(1)} %maximum_maximum_fusion.gd_ref) | copy-start | bytes 24580
  37.1 97.0 %copy-start = (bf16[64,2048]{1,0:T(8,128)(2,1)S(1)}, bf16[64,2048]{1,0:T(8,128)(2,1)}, u32[]{:S(2)}) copy-start(bf16[64,2048]{1,0:T(8,128)(2,1)} %get-tuple-element.7) | copy-start | bytes 786436
